TPU v7x, 32 devices: a whole 2x2x4 slice. The times are simulated.
32 devices in a mesh: ep: 8 (over z, core), tp: 4 (over y, x).
Axes of the slice: x: 2, y: 2, z: 4, core: 2. Of those that a mesh axis runs over, the one named last changes fastest.
Arguments:
- query_rows: bfloat16 [3072, 2048], P('ep', 'tp'), may hold values from -6 to 6
- key_rows: bfloat16 [3072, 2048], P('ep', 'tp'), may hold values from -6 to 6
- value_rows: bfloat16 [3072, 2048], P('ep', 'tp'), may hold values from -6 to 6
- second_scale: float32 [16], P('tp'), may hold values from 0.3 to 0.8
- head_gain: float32 [128], replicated, may hold values from 0.1 to 1.9
- out_weight: bfloat16 [2048, 4096], P(None, 'tp'), may hold values from -0.125 to 0.125
- routed_rows: bfloat16 [1024, 4096], P('ep', 'tp'), may hold values from -6 to 6
- norm_gain: float32 [4096], replicated, may hold values from 0.1 to 1.9
- route_ids: int32 [1024, 2], P('ep'), may hold values from 0 to 7, all different within a row; in each aligned block of 128 rows (0 to 127, 128 to 255, ...) at most 64 rows name the same one
- route_weight: float32 [1024, 2], P('ep'), may hold values from 0.1 to 0.9
- expert_gate: bfloat16 [8, 4096, 2048], P('ep', None, 'tp'), may hold values from -0.09375 to 0.09375
- expert_up: bfloat16 [8, 4096, 2048], P('ep', None, 'tp'), may hold values from -0.09375 to 0.09375
- expert_down: bfloat16 [8, 2048, 4096], P('ep', None, 'tp'), may hold values from -0.125 to 0.125
Outputs:
- mixer_out: bfloat16 [3072, 4096], P('ep', 'tp')
- expert_mix: bfloat16 [1024, 4096], P('ep', 'tp')
Inputs may be any that keep to these rules, and one draw needn't show every extreme that they name: `route_ids`: among the 128 tokens of one index of ep, no expert is named by more than 64 of them, a bound that some block reaches.
All inputs are finite; a program needn't handle non-finite values.
Results may differ from a plain program's by a relative error of at most 0.0085.
Values may be sent and summed in bfloat16 or wider, within the bound.
No kernel may reach another device: no remote copies, remote signals or barrier semaphores. Data moves between devices by JAX's collectives and lax.ppermute only.
A program may use at most 128 MiB of HBM per device.

v0:
```python
import jax
import jax.numpy as jnp
from jax import lax
from jax.sharding import PartitionSpec as P

eps = 1e-06
head_factor = 0.8
neg_big = -1e30
key_block_rows = 1024


def rms_rows(rows_in, gain):
    floats = rows_in.astype(jnp.float32)
    factor = lax.rsqrt(jnp.mean(floats * floats, axis=-1, keepdims=True) + eps)
    return (floats * factor * gain).astype(jnp.bfloat16)


def per_device(
    query_rows,
    key_rows,
    value_rows,
    second_scale,
    head_gain,
    out_weight,
    routed_rows,
    norm_gain,
    route_ids,
    route_weight,
    expert_gate,
    expert_up,
    expert_down,
):
    count_a = query_rows.shape[0]
    per_head = second_scale.shape[0]
    head_dim = query_rows.shape[1] // (2 * per_head)
    value_dim = head_gain.shape[0]
    query_four = query_rows.reshape(count_a, per_head, 2, head_dim)
    query_pos = lax.axis_index("ep") * count_a + jnp.arange(count_a, dtype=jnp.int32)

    def key_block(carry_state, key_part, value_part, block_start):
        key_count = key_part.shape[0]
        key_four = key_part.reshape(key_count, per_head, 2, head_dim)
        value_three = value_part.reshape(key_count, per_head, value_dim)
        scores = jnp.einsum(
            "ihcd,jhcd->ihcj", query_four, key_four, preferred_element_type=jnp.float32
        ) * head_dim ** (-0.5)
        allowed = (
            query_pos[:, None] >= block_start + jnp.arange(key_count, dtype=jnp.int32)[None, :]
        )[:, None, None, :]
        scores = jnp.where(allowed, scores, neg_big)
        old_max, old_sum, old_acc = carry_state
        new_max = jnp.maximum(old_max, jnp.max(scores, axis=-1))
        weights = jnp.where(allowed, jnp.exp(scores - new_max[..., None]), 0.0)
        shrink = jnp.exp(old_max - new_max)
        new_sum = old_sum * shrink + jnp.sum(weights, axis=-1)
        update = jnp.einsum(
            "ihcj,jhe->ihce",
            weights.astype(jnp.bfloat16),
            value_three,
            preferred_element_type=jnp.float32,
        )
        return (new_max, new_sum, old_acc * shrink[..., None] + update)

    start_state = (
        jnp.full((count_a, per_head, 2), neg_big, jnp.float32),
        jnp.zeros((count_a, per_head, 2), jnp.float32),
        jnp.zeros((count_a, per_head, 2, value_dim), jnp.float32),
    )
    key_part = lax.all_gather(key_rows, "ep", axis=0, tiled=True)
    value_part = lax.all_gather(value_rows, "ep", axis=0, tiled=True)
    key_count = key_part.shape[0]

    def step_block(block_num, inner_state):
        offset_rows = block_num * key_block_rows
        key_slice = lax.dynamic_slice_in_dim(key_part, offset_rows, key_block_rows, 0)
        value_slice = lax.dynamic_slice_in_dim(value_part, offset_rows, key_block_rows, 0)
        return key_block(inner_state, key_slice, value_slice, offset_rows)

    run_max, run_sum, run_acc = lax.fori_loop(
        0, key_count // key_block_rows, step_block, start_state
    )
    maps_both = run_acc / run_sum[..., None]
    mixed_maps = maps_both[:, :, 0] - second_scale[None, :, None] * maps_both[:, :, 1]
    mean_sq = jnp.mean(mixed_maps * mixed_maps, axis=-1, keepdims=True)
    head_out = (
        (mixed_maps * lax.rsqrt(mean_sq + eps) * head_gain * head_factor)
        .astype(jnp.bfloat16)
        .reshape(count_a, per_head * value_dim)
    )
    count_b = routed_rows.shape[0]
    route_count = route_ids.shape[1]
    experts_here = expert_gate.shape[0]
    ep_devices = lax.axis_size("ep")
    expert_total = experts_here * ep_devices
    capacity = 2 * count_b * route_count // expert_total
    flat_expert = route_ids.reshape(-1)
    chosen = (flat_expert[:, None] == jnp.arange(expert_total, dtype=jnp.int32)[None, :]).astype(
        jnp.int32
    )
    ranks = jnp.sum((jnp.cumsum(chosen, axis=0) - 1) * chosen, axis=1)
    slot_of = flat_expert * capacity + ranks
    token_of = jnp.arange(count_b * route_count, dtype=jnp.int32) // route_count
    slot_token = jnp.full((expert_total * capacity,), count_b, jnp.int32).at[slot_of].set(token_of)
    padded = jnp.concatenate(
        [routed_rows, jnp.zeros((1, routed_rows.shape[1]), jnp.bfloat16)], axis=0
    )
    outgoing = padded[slot_token].reshape(ep_devices, experts_here, capacity, routed_rows.shape[1])
    column_parts = lax.all_to_all(outgoing, "ep", split_axis=0, concat_axis=0, tiled=True)
    arrived = rms_rows(lax.all_gather(column_parts, "tp", axis=3, tiled=True), norm_gain)
    gate_val = jnp.einsum(
        "sxcd,xdf->sxcf", arrived, expert_gate, preferred_element_type=jnp.float32
    )
    up_val = jnp.einsum("sxcd,xdf->sxcf", arrived, expert_up, preferred_element_type=jnp.float32)
    hidden = (jax.nn.silu(gate_val) * up_val).astype(jnp.bfloat16)
    weight_rows = out_weight
    attn_total = jnp.dot(
        lax.all_gather(
            head_out.reshape(1, 1, count_a, head_out.shape[1]), "tp", axis=3, tiled=True
        )[0, 0],
        weight_rows,
        preferred_element_type=jnp.float32,
    )
    weight_rows = expert_down
    moe_total = jnp.einsum(
        "sxcf,xfd->sxcd",
        lax.all_gather(hidden, "tp", axis=3, tiled=True),
        weight_rows,
        preferred_element_type=jnp.float32,
    )
    mixer_out = attn_total.astype(jnp.bfloat16)
    returned = lax.all_to_all(
        moe_total.astype(jnp.bfloat16), "ep", split_axis=0, concat_axis=0, tiled=True
    )
    flat_back = returned.reshape(expert_total * capacity, returned.shape[3])
    picked = flat_back[slot_of].astype(jnp.float32).reshape(count_b, route_count, returned.shape[3])
    expert_mix = jnp.sum(picked * route_weight[:, :, None], axis=1).astype(jnp.bfloat16)
    return (mixer_out, expert_mix)


def solution(mesh):
    placed = (
        P("ep", "tp"),
        P("ep", "tp"),
        P("ep", "tp"),
        P("tp"),
        P(),
        P(None, "tp"),
        P("ep", "tp"),
        P(),
        P("ep", None),
        P("ep", None),
        P("ep", None, "tp"),
        P("ep", None, "tp"),
        P("ep", None, "tp"),
    )
    return jax.shard_map(
        per_device,
        mesh=mesh,
        in_specs=placed,
        out_specs=(P("ep", "tp"), P("ep", "tp")),
        check_vma=False,
    )
```

profile of v0, /device:TPU:0, one launch (start us, length us, event | category | flops | bytes accessed | tf_op | source)
XLA Modules:
  0.0 287.7 jit_solution(6418652989304294273)
XLA Ops:
  12.6 2.1 gather_fusion
  14.7 33.0 %all_to_all.10 = bf16[8,1,64,1024]{3,2,1,0:T(8,128)(2,1)} all-to-all(bf16[8,1,64,1024]{3,2,1,0:T(8,128)(2,1)S(1)} %bitcast.152), channel_id=1, replica_groups=mesh['ep'=8,'tp'=4] {'ep'}, dimensions={0} | all-to-all | bytes 2097152 | tf_op jit(solution)/shard_map/all_to_all | solution.py:108
  51.1 48.2 %all-gather.12.cloned.1.call-done = bf16[8,1,64,4096]{3,2,1,0:T(8,128)(2,1)} async-done(((bf16[8,1,64,1024]{3,2,1,0:T(8,128)(2,1)}), bf16[8,1,64,4096]{3,2,1,0:T(8,128)(2,1)}) %all-gather.12.cloned.1.call-update) | async-done | bytes 4194320 | tf_op jit(solution)/shard_map/all_gather | solution.py:109
  99.4 3.2 %fusion.15 = f32[8,64]{1,0:T(8,128)S(1)} fusion(bf16[8,1,64,4096]{3,2,1,0:T(8,128)(2,1)} %all-gather.12.cloned.1.call-done), kind=kLoop, calls=%fused_computation.28 | loop fusion | flops 6290944 | bytes 4196352 | tf_op jit(solution)/shard_map/reduce_sum | solution.py:14
  102.8 4.7 %fusion.43 = f32[8,1,64,512]{3,2,0,1:T(8,128)S(1)} fusion(bf16[1,4096,512]{2,1,0:T(8,128)(2,1)} %param.25, bf16[8,1,64,4096]{3,2,1,0:T(8,128)(2,1)S(1)} %copy-done.1, f32[4096]{0:T(1024)S(1)} %copy-done.8, f32[8,64]{1,0:T(8,128)S(1)} %add_rsqrt_fusion.1), kind=kOutput, calls=%fused_computation.44 | convolution fusion | flops 2155872256 | bytes 9455616 | tf_op jit(solution)/shard_map/sxcd,xdf->sxcf/dot_general | solution.py:110
  107.5 3.3 %fusion.58 = bf16[8,1,64,512]{3,2,0,1:T(8,128)(2,1)} fusion(bf16[1,4096,512]{2,1,0:T(8,128)(2,1)S(1)} %copy-done.7, bf16[8,1,64,4096]{3,2,1,0:T(8,128)(2,1)S(1)} %copy-done.1, f32[4096]{0:T(1024)S(1)} %copy-done.8, f32[8,64]{1,0:T(8,128)S(1)} %add_rsqrt_fusion.1, f32[8,1,64,512]{3,2,0,1:T(8,128)S(1)} %fusion.43), kind=kOutput, calls=%fused_computation.47 | convolution fusion | flops 2157445120 | bytes 9979904 | tf_op jit(solution)/shard_map/sxcd,xdf->sxcf/dot_general | solution.py:113
  111.0 27.7 %all-gather.6.cloned.1.call-done = bf16[3072,512]{0,1:T(8,128)(2,1)} async-done(((bf16[384,512]{0,1:T(8,128)(2,1)}), bf16[3072,512]{0,1:T(8,128)(2,1)}) %all-gather.6.cloned.1.call-update) | async-done | bytes 3145744 | tf_op jit(solution)/shard_map/all_gather | solution.py:69
  138.8 38.8 %all-gather.8.cloned.1.call-done = bf16[3072,512]{0,1:T(8,128)(2,1)} async-done(((bf16[384,512]{0,1:T(8,128)(2,1)}), bf16[3072,512]{0,1:T(8,128)(2,1)}) %all-gather.8.cloned.1.call-update) | async-done | bytes 3145744 | tf_op jit(solution)/shard_map/all_gather | solution.py:70
  177.5 61.9 %while.18 = (s32[]{:T(128)}, f32[384,4,2]{0,2,1:T(2,128)S(1)}, f32[384,4,2]{0,2,1:T(2,128)S(1)}, f32[384,4,2,128]{0,3,2,1:T(8,128)S(1)}, bf16[3072,512]{0,1:T(8,...) while((s32[]{:T(128)}, f32[384,4,2]{0,2,1:T(2,128)S(1)}, ...), condition=%wide.region_3.4_spmd.clone, body=%wide.region_0.3_spmd.clone.sunk | while | flops 1250443648 | bytes 99691744 | solution.py:79
  177.8 1.7 constant_dynamic-slice_fusion.3
  179.5 6.7 %fusion.86 = (f32[384,4,2]{0,2,1:T(2,128)S(1)}, f32[4,2,1024,384]{3,2,1,0:T(8,128)}) fusion(pred[384,1024]{0,1:T(8,128)(4,1)S(1)} %broadcast_compare_fusion.2, bf16[1024,4,2,64]{0,3,2,1:T(8,128)(2,1)S(1)} %bitcast.148, bf16[384,4,2,64]{0,3,2,1:T(8,128)(2,1)S(1)} %get-tuple-element.290), kind=kOutput, calls=%fused_computation.6.clone.1 | convolution fusion | flops 412087296 | bytes 14430208 | tf_op jit(solution)/shard_map/while/body/eval_jaxpr/ihcd,jhcd->ihcj/dot_general | solution.py:44
  186.2 7.0 %fusion.88 = f32[384,4,2]{0,2,1:T(2,128)S(1)} fusion(f32[4,2,1024,384]{3,2,1,0:T(8,128)} %get-tuple-element.257, f32[384,4,2]{0,2,1:T(2,128)S(1)} %fusion.87, pred[384,1024]{0,1:T(8,128)(4,1)S(1)} %broadcast_compare_fusion.2), kind=kLoop, calls=%fused_computation.8.clone.1 | loop fusion | flops 15725568 | bytes 13000704 | tf_op jit(solution)/shard_map/while/body/eval_jaxpr/reduce_sum | solution.py:55
  194.7 3.6 %bitcast_add_fusion.2 = f32[384,4,2,128]{0,3,2,1:T(8,128)S(1)} fusion(f32[384,4,2,128]{0,3,2,1:T(8,128)S(1)} %get-tuple-element.276, bf16[1024,4,128,1]{0,2,3,1:T(8,128)(2,1)S(1)} %bitcast.149, f32[4,2,1024,384]{3,2,1,0:T(8,128)S(1)} %copy-done, f32[384,4,2]{0,2,1:T(2,128)S(1)} %fusion.87, pred[384,1024]{0,1:T(8,128)(4,1)S(1)} %broadcast_compare_fusion.2, ...), kind=kOutput, calls=%fused_computation.11.clone.1 | convolution fusion | flops 822214656 | bytes 17195008 | tf_op jit(solution)/shard_map/while/body/eval_jaxpr/ihcj,jhe->ihce/dot_general | solution.py:56
  200.3 6.7 %fusion.86 = (f32[384,4,2]{0,2,1:T(2,128)S(1)}, f32[4,2,1024,384]{3,2,1,0:T(8,128)}) fusion(pred[384,1024]{0,1:T(8,128)(4,1)S(1)} %broadcast_compare_fusion.2, bf16[1024,4,2,64]{0,3,2,1:T(8,128)(2,1)S(1)} %bitcast.148, bf16[384,4,2,64]{0,3,2,1:T(8,128)(2,1)S(1)} %get-tuple-element.290), kind=kOutput, calls=%fused_computation.6.clone.1 | convolution fusion | flops 412087296 | bytes 14430208 | tf_op jit(solution)/shard_map/while/body/eval_jaxpr/ihcd,jhcd->ihcj/dot_general | solution.py:44
  207.0 6.8 %fusion.88 = f32[384,4,2]{0,2,1:T(2,128)S(1)} fusion(f32[4,2,1024,384]{3,2,1,0:T(8,128)} %get-tuple-element.257, f32[384,4,2]{0,2,1:T(2,128)S(1)} %fusion.87, pred[384,1024]{0,1:T(8,128)(4,1)S(1)} %broadcast_compare_fusion.2), kind=kLoop, calls=%fused_computation.8.clone.1 | loop fusion | flops 15725568 | bytes 13000704 | tf_op jit(solution)/shard_map/while/body/eval_jaxpr/reduce_sum | solution.py:55
  215.3 3.6 %bitcast_add_fusion.2 = f32[384,4,2,128]{0,3,2,1:T(8,128)S(1)} fusion(f32[384,4,2,128]{0,3,2,1:T(8,128)S(1)} %get-tuple-element.276, bf16[1024,4,128,1]{0,2,3,1:T(8,128)(2,1)S(1)} %bitcast.149, f32[4,2,1024,384]{3,2,1,0:T(8,128)S(1)} %copy-done, f32[384,4,2]{0,2,1:T(2,128)S(1)} %fusion.87, pred[384,1024]{0,1:T(8,128)(4,1)S(1)} %broadcast_compare_fusion.2, ...), kind=kOutput, calls=%fused_computation.11.clone.1 | convolution fusion | flops 822214656 | bytes 17195008 | tf_op jit(solution)/shard_map/while/body/eval_jaxpr/ihcj,jhe->ihce/dot_general | solution.py:56
  220.9 6.7 %fusion.86 = (f32[384,4,2]{0,2,1:T(2,128)S(1)}, f32[4,2,1024,384]{3,2,1,0:T(8,128)}) fusion(pred[384,1024]{0,1:T(8,128)(4,1)S(1)} %broadcast_compare_fusion.2, bf16[1024,4,2,64]{0,3,2,1:T(8,128)(2,1)S(1)} %bitcast.148, bf16[384,4,2,64]{0,3,2,1:T(8,128)(2,1)S(1)} %get-tuple-element.290), kind=kOutput, calls=%fused_computation.6.clone.1 | convolution fusion | flops 412087296 | bytes 14430208 | tf_op jit(solution)/shard_map/while/body/eval_jaxpr/ihcd,jhcd->ihcj/dot_general | solution.py:44
  227.6 6.8 %fusion.88 = f32[384,4,2]{0,2,1:T(2,128)S(1)} fusion(f32[4,2,1024,384]{3,2,1,0:T(8,128)} %get-tuple-element.257, f32[384,4,2]{0,2,1:T(2,128)S(1)} %fusion.87, pred[384,1024]{0,1:T(8,128)(4,1)S(1)} %broadcast_compare_fusion.2), kind=kLoop, calls=%fused_computation.8.clone.1 | loop fusion | flops 15725568 | bytes 13000704 | tf_op jit(solution)/shard_map/while/body/eval_jaxpr/reduce_sum | solution.py:55
  235.9 3.6 %bitcast_add_fusion.2 = f32[384,4,2,128]{0,3,2,1:T(8,128)S(1)} fusion(f32[384,4,2,128]{0,3,2,1:T(8,128)S(1)} %get-tuple-element.276, bf16[1024,4,128,1]{0,2,3,1:T(8,128)(2,1)S(1)} %bitcast.149, f32[4,2,1024,384]{3,2,1,0:T(8,128)S(1)} %copy-done, f32[384,4,2]{0,2,1:T(2,128)S(1)} %fusion.87, pred[384,1024]{0,1:T(8,128)(4,1)S(1)} %broadcast_compare_fusion.2, ...), kind=kOutput, calls=%fused_computation.11.clone.1 | convolution fusion | flops 822214656 | bytes 17195008 | tf_op jit(solution)/shard_map/while/body/eval_jaxpr/ihcj,jhe->ihce/dot_general | solution.py:56
  241.0 6.1 %fusion.38 = bf16[8,1,64,1024]{3,2,1,0:T(8,128)(2,1)} fusion(bf16[1,2048,1024]{2,1,0:T(8,128)(2,1)} %param.27, bf16[8,1,64,2048]{3,2,0,1:T(8,128)(2,1)} %all-gather.14.cloned.1.call-done), kind=kOutput, calls=%fused_computation.43 | convolution fusion | flops 2148007936 | bytes 7340032 | tf_op jit(solution)/shard_map/sxcf,xfd->sxcd/dot_general | solution.py:124
  247.2 3.6 %all-to-all-start.1 = ((bf16[8,1,64,1024]{3,2,1,0:T(8,128)(2,1)}), bf16[8,1,64,1024]{3,2,1,0:T(8,128)(2,1)S(1)}, u32[]{:S(2)}, u32[]{:S(2)}) async-start(bf16[8,1,64,1024]{3,2,1,0:T(8,128)(2,1)} %fusion.38), calls=%async_computation.1 | async-start | bytes 2097152 | tf_op jit(solution)/shard_map/all_to_all | solution.py:131
  250.9 20.8 %all-gather.10.cloned.1.call-done = bf16[1,1,384,2048]{2,3,1,0:T(8,128)(2,1)} async-done(((bf16[1,1,384,512]{2,3,1,0:T(8,128)(2,1)}), bf16[1,1,384,2048]{2,3,1,0:T(8,128)(2,1)}) %all-gather.10.cloned.1.call-update) | async-done | bytes 1572880 | tf_op jit(solution)/shard_map/all_gather | solution.py:117
  271.6 5.4 %fusion.35 = bf16[384,1024]{1,0:T(8,128)(2,1)} fusion(bf16[2048,1024]{1,0:T(8,128)(2,1)} %param.20, bf16[1,1,384,2048]{2,3,1,0:T(8,128)(2,1)} %all-gather.10.cloned.1.call-done), kind=kOutput, calls=%fused_computation.42 | convolution fusion | flops 1611005952 | bytes 6553600 | tf_op jit(solution)/shard_map/dot_general | solution.py:116
  279.0 2.1 multiply_reduce_fusion
  (90 shorter events, 21.7 us)
Async XLA Ops:
  7.2 92.2 %all-gather.12.cloned.1.call-start = ((), (), s32[]{:S(2)}) async-start(), calls=%async_computation.5 | async-start | bytes 5242880 | tf_op jit(solution)/shard_map/all_gather | solution.py:109
  12.6 35.1 %copy-start.2 = (bf16[384,512]{1,0:T(8,128)(2,1)S(1)}, bf16[384,512]{1,0:T(8,128)(2,1)}, u32[]{:S(2)}) copy-start(bf16[384,512]{1,0:T(8,128)(2,1)} %param.16) | copy-start | bytes 1179652
  14.7 34.1 %copy-start.3 = (bf16[384,512]{1,0:T(8,128)(2,1)S(1)}, bf16[384,512]{1,0:T(8,128)(2,1)}, u32[]{:S(2)}) copy-start(bf16[384,512]{1,0:T(8,128)(2,1)} %param.17) | copy-start | bytes 1179652
  14.7 36.3 %copy-start.4 = (f32[4]{0:T(128)S(1)}, f32[4]{0:T(128)}, u32[]{:S(2)}) copy-start(f32[4]{0:T(128)} %param.18) | copy-start | bytes 52
  14.7 36.3 %copy-start.6 = (f32[128]{0:T(128)S(1)}, f32[128]{0:T(128)}, u32[]{:S(2)}) copy-start(f32[128]{0:T(128)} %param.19) | copy-start | bytes 1540
  47.7 54.9 %copy-start.8 = (f32[4096]{0:T(1024)S(1)}, f32[4096]{0:T(1024)}, u32[]{:S(2)}) copy-start(f32[4096]{0:T(1024)} %param.22) | copy-start | bytes 49156
  47.7 91.1 %all-gather.6.cloned.1.call-start = ((), (), s32[]{:S(2)}) async-start(), calls=%async_computation.2 | async-start | bytes 3538944 | tf_op jit(solution)/shard_map/all_gather | solution.py:69
  48.7 128.8 %all-gather.8.cloned.1.call-start = ((), (), s32[]{:S(2)}) async-start(), calls=%async_computation.3 | async-start | bytes 3538944 | tf_op jit(solution)/shard_map/all_gather | solution.py:70
  49.7 191.3 %all-gather.14.cloned.1.call-start = ((), (), s32[]{:S(2)}) async-start(), calls=%async_computation.6 | async-start | bytes 2621440 | tf_op jit(solution)/shard_map/all_gather | solution.py:126
  99.3 3.4 %copy-start.1 = (bf16[8,1,64,4096]{3,2,1,0:T(8,128)(2,1)S(1)}, bf16[8,1,64,4096]{3,2,1,0:T(8,128)(2,1)}, u32[]{:S(2)}) copy-start(bf16[8,1,64,4096]{3,2,1,0:T(8,128)(2,1)} %all-gather.12.cloned.1.call-done) | copy-start | bytes 12582916
  102.8 4.7 %copy-start.7 = (bf16[1,4096,512]{2,1,0:T(8,128)(2,1)S(1)}, bf16[1,4096,512]{2,1,0:T(8,128)(2,1)}, u32[]{:S(2)}) copy-start(bf16[1,4096,512]{2,1,0:T(8,128)(2,1)} %param.26) | copy-start | bytes 12582916
  110.8 160.8 %all-gather.10.cloned.1.call-start = ((), (), s32[]{:S(2)}) async-start(), calls=%async_computation.4 | async-start | bytes 1966080 | tf_op jit(solution)/shard_map/all_gather | solution.py:117
  186.2 8.5 %copy-start = (f32[4,2,1024,384]{3,2,1,0:T(8,128)S(1)}, f32[4,2,1024,384]{3,2,1,0:T(8,128)}, u32[]{:S(2)}) copy-start(f32[4,2,1024,384]{3,2,1,0:T(8,128)} %get-tuple-element.257) | copy-start | bytes 37748740 | tf_op jit(solution)/shard_map/while
  207.0 8.3 %copy-start = (f32[4,2,1024,384]{3,2,1,0:T(8,128)S(1)}, f32[4,2,1024,384]{3,2,1,0:T(8,128)}, u32[]{:S(2)}) copy-start(f32[4,2,1024,384]{3,2,1,0:T(8,128)} %get-tuple-element.257) | copy-start | bytes 37748740 | tf_op jit(solution)/shard_map/while
  227.6 8.3 %copy-start = (f32[4,2,1024,384]{3,2,1,0:T(8,128)S(1)}, f32[4,2,1024,384]{3,2,1,0:T(8,128)}, u32[]{:S(2)}) copy-start(f32[4,2,1024,384]{3,2,1,0:T(8,128)} %get-tuple-element.257) | copy-start | bytes 37748740 | tf_op jit(solution)/shard_map/while
  241.0 9.7 %copy-start.5 = (f32[128,2]{0,1:T(2,128)S(1)}, f32[128,2]{0,1:T(2,128)}, u32[]{:S(2)}) copy-start(f32[128,2]{0,1:T(2,128)} %param.24) | copy-start | bytes 3076
  247.2 30.1 %all-to-all-start.1 = ((bf16[8,1,64,1024]{3,2,1,0:T(8,128)(2,1)}), bf16[8,1,64,1024]{3,2,1,0:T(8,128)(2,1)S(1)}, u32[]{:S(2)}, u32[]{:S(2)}) async-start(bf16[8,1,64,1024]{3,2,1,0:T(8,128)(2,1)} %fusion.38), calls=%async_computation.1 | async-start | bytes 2097152 | tf_op jit(solution)/shard_map/all_to_all | solution.py:131
Sparse Core Ops, SparseCore 0:
  47.8 51.4 all-gather.11
  101.0 37.7 all-gather.5
  140.4 37.0 all-gather.7
  179.8 34.3 all-gather.13
  241.1 30.4 all-gather.9
where the time goes:
time: 288 us
  waiting for transfers between devices  136 us (47%)
  matrix products  50.1 us (17%)
  blocking collectives  33 us (11%)
  other arithmetic  29.5 us (10%)
  local copies, waits for them, and re-layouts  21 us (7%)
  between operations  14 us (5%)
  starting transfers between devices  3.94 us (1%)
    all_gather x1, waiting for transfers between devices, per_device(): lax.all_gather(column_parts, 'tp', axis=3, tiled=True)  48.2 us
    all_gather x1, waiting for transfers between devices, per_device(): value_part = lax.all_gather(value_rows, 'ep', axis=0, tiled=True)  38.8 us
    all_to_all x1, blocking collectives, per_device(): lax.all_to_all(outgoing, 'ep', split_axis=0, concat_axis=0, tiled=True)  33 us
    all_gather x1, waiting for transfers between devices, per_device(): key_part = lax.all_gather(key_rows, 'ep', axis=0, tiled=True)  27.7 us
    all_gather x1, waiting for transfers between devices, per_device(): lax.all_gather(head_out.reshape(1, 1, count_a, head_out.shape[1]), 'tp',...  20.8 us
    reduce_sum x3, other arithmetic, key_block(): new_sum = old_sum * shrink + jnp.sum(weights, axis=-1)  20.5 us
    dot_general x3, matrix products, key_block(): jnp.einsum('ihcd,jhcd->ihcj', query_four, key_four, preferred_element_typ...  20 us
    dot_general x3, matrix products, key_block(): jnp.einsum('ihcj,jhe->ihce', weights.astype(jnp.bfloat16), value_three, p...  10.7 us
  transfers between devices with their start and end apart: 6, of which 5 were waited for; matrix products, arithmetic and copies ran while one was open for 29% of the time, Pallas kernels for 0%

commit v1 on v0

--- a/solution.py
+++ b/solution.py
@@ -67,7 +67,20 @@
         jnp.zeros((count_a, per_head, 2, value_dim), jnp.float32),
     )
     key_part = lax.all_gather(key_rows, "ep", axis=0, tiled=True)
-    value_part = lax.all_gather(value_rows, "ep", axis=0, tiled=True)
+
+    def find_area_here(view, mesh_name):
+        axis_n = lax.axis_size(mesh_name)
+        formed = sorted(((w, (w + 1) % axis_n) for w in range(axis_n)))
+        upper = view
+        samples = [upper]
+        for it in tuple(range(1, axis_n)):
+            upper = lax.ppermute(upper, mesh_name, formed)
+            samples.insert(0, upper)
+        piece_now = jnp.concatenate(samples, 0)
+        block_now = lax.axis_index(mesh_name) + 1
+        return jnp.roll(piece_now, block_now * view.shape[0], 0)
+
+    value_part = find_area_here(value_rows, "ep")
     key_count = key_part.shape[0]
 
     def step_block(block_num, inner_state):

time: 288 us -> 250 us (0.87)
  waiting for transfers between devices: 136 us -> 83.4 us
  local copies, waits for them, and re-layouts: 21 us -> 33.3 us
    ppermute x0 -> x7, waiting for transfers between devices: none -> 61.1 us  [find_area_here(): upper = lax.ppermute(upper, mesh_name, formed)]
    all_gather x1, waiting for transfers between devices: 48.2 us -> 0.01 us  [per_device(): lax.all_gather(column_parts, 'tp', axis=3, tiled=True)]
    all_gather x1 -> x0, waiting for transfers between devices: 38.8 us -> none  [per_device(): value_part = lax.all_gather(value_rows, 'ep', axis=0, tiled=True)]
    all_gather x1, waiting for transfers between devices: 27.7 us -> 1.25 us  [per_device(): key_part = lax.all_gather(key_rows, 'ep', axis=0, tiled=True)]
    unnamed x21 -> x48, local copies, waits for them, and re-layouts: 4.21 us -> 12.4 us
    dynamic_slice x0 -> x1, local copies, waits for them, and re-layouts: none -> 4.08 us  [find_area_here(): return jnp.roll(piece_now, block_now * view.shape[0], 0)]
  transfers between devices with their start and end apart: 6 -> 12, of which waited for: 5 -> 10; matrix products, arithmetic and copies ran while one was open for 29% -> 39% of each run, Pallas kernels for 0% -> 0%
where the time goes in v1:
time: 250 us; the launch traced here: 249 us
  waiting for transfers between devices  83.4 us (33%)
  matrix products  51.4 us (21%)
  local copies, waits for them, and re-layouts  33.3 us (13%)
  blocking collectives  32.8 us (13%)
  other arithmetic  29.4 us (12%)
  between operations  14.2 us (6%)
  starting transfers between devices  4.01 us (2%)
    ppermute x7, waiting for transfers between devices, find_area_here(): upper = lax.ppermute(upper, mesh_name, formed)  61.1 us
    all_to_all x1, blocking collectives, per_device(): lax.all_to_all(outgoing, 'ep', split_axis=0, concat_axis=0, tiled=True)  32.8 us
    all_gather x1, waiting for transfers between devices, per_device(): lax.all_gather(head_out.reshape(1, 1, count_a, head_out.shape[1]), 'tp',...  20.6 us
    reduce_sum x3, other arithmetic, key_block(): new_sum = old_sum * shrink + jnp.sum(weights, axis=-1)  20.5 us
    dot_general x3, matrix products, key_block(): jnp.einsum('ihcd,jhcd->ihcj', query_four, key_four, preferred_element_typ...  19.9 us
    unnamed x48, local copies, waits for them, and re-layouts  12.4 us
    dot_general x3, matrix products, key_block(): jnp.einsum('ihcj,jhe->ihce', weights.astype(jnp.bfloat16), value_three, p...  10.7 us
    dot_general x1, matrix products, per_device(): jnp.einsum('sxcf,xfd->sxcd', lax.all_gather(hidden, 'tp', axis=3, tiled=T...  6.14 us
  transfers between devices with their start and end apart: 12, of which 10 were waited for; matrix products, arithmetic and copies ran while one was open for 39% of the time, Pallas kernels for 0%

profile of v1, /device:TPU:0, one launch (start us, length us, event | category | flops | bytes accessed | tf_op | source)
XLA Modules:
  0.0 248.9 jit_solution(13829101176312967507)
XLA Ops:
  14.7 32.8 %all_to_all.10 = bf16[8,1,64,1024]{3,2,1,0:T(8,128)(2,1)} all-to-all(bf16[8,1,64,1024]{3,2,1,0:T(8,128)(2,1)S(1)} %bitcast.152), channel_id=1, replica_groups=mesh['ep'=8,'tp'=4] {'ep'}, dimensions={0} | all-to-all | bytes 2097152 | tf_op jit(solution)/shard_map/all_to_all | solution.py:121
  47.9 9.0 %collective-permute-done = bf16[384,512]{0,1:T(8,128)(2,1)S(1)} collective-permute-done((bf16[384,512]{0,1:T(8,128)(2,1)S(1)}, bf16[384,512]{0,1:T(8,128)(2,1)S(1)}, u32[]{:S(2)}, u32[]{:S(2)}) %collective-permute-start) | collective-permute-done | bytes 393248 | tf_op jit(solution)/shard_map/ppermute | solution.py:77
  56.9 9.0 %collective-permute-done.1 = bf16[384,512]{0,1:T(8,128)(2,1)S(1)} collective-permute-done((bf16[384,512]{0,1:T(8,128)(2,1)S(1)}, bf16[384,512]{0,1:T(8,128)(2,1)S(1)}, u32[]{:S(2)}, u32[]{:S(2)}) %collective-permute-start.1) | collective-permute-done | bytes 393248 | tf_op jit(solution)/shard_map/ppermute | solution.py:77
  65.9 9.0 %collective-permute-done.2 = bf16[384,512]{0,1:T(8,128)(2,1)S(1)} collective-permute-done((bf16[384,512]{0,1:T(8,128)(2,1)S(1)}, bf16[384,512]{0,1:T(8,128)(2,1)S(1)}, u32[]{:S(2)}, u32[]{:S(2)}) %collective-permute-start.2) | collective-permute-done | bytes 393248 | tf_op jit(solution)/shard_map/ppermute | solution.py:77
  75.6 9.0 %collective-permute-done.3 = bf16[384,512]{0,1:T(8,128)(2,1)S(1)} collective-permute-done((bf16[384,512]{0,1:T(8,128)(2,1)S(1)}, bf16[384,512]{0,1:T(8,128)(2,1)S(1)}, u32[]{:S(2)}, u32[]{:S(2)}) %collective-permute-start.3) | collective-permute-done | bytes 393248 | tf_op jit(solution)/shard_map/ppermute | solution.py:77
  85.6 8.0 %collective-permute-done.4 = bf16[384,512]{0,1:T(8,128)(2,1)S(1)} collective-permute-done((bf16[384,512]{0,1:T(8,128)(2,1)S(1)}, bf16[384,512]{0,1:T(8,128)(2,1)S(1)}, u32[]{:S(2)}, u32[]{:S(2)}) %collective-permute-start.4) | collective-permute-done | bytes 393248 | tf_op jit(solution)/shard_map/ppermute | solution.py:77
  93.6 9.1 %collective-permute-done.5 = bf16[384,512]{0,1:T(8,128)(2,1)} collective-permute-done((bf16[384,512]{0,1:T(8,128)(2,1)S(1)}, bf16[384,512]{0,1:T(8,128)(2,1)}, u32[]{:S(2)}, u32[]{:S(2)}) %collective-permute-start.5) | collective-permute-done | bytes 393248 | tf_op jit(solution)/shard_map/ppermute | solution.py:77
  104.1 8.0 %collective-permute-done.6 = bf16[384,512]{0,1:T(8,128)(2,1)} collective-permute-done((bf16[384,512]{0,1:T(8,128)(2,1)}, bf16[384,512]{0,1:T(8,128)(2,1)}, u32[]{:S(2)}, u32[]{:S(2)}) %collective-permute-start.6) | collective-permute-done | bytes 393248 | tf_op jit(solution)/shard_map/ppermute | solution.py:77
  120.7 4.1 %constant_dynamic-slice_fusion.2 = bf16[3072,512]{0,1:T(8,128)(2,1)} fusion(bf16[6144,512]{0,1:T(8,128)(2,1)S(1)} %constant_dynamic-update-slice_fusion, s32[]{:T(128)S(6)} %select_n.56), kind=kLoop, calls=%fused_computation.92 | loop fusion | bytes 6291460 | tf_op jit(solution)/shard_map/jit(_roll_dynamic)/dynamic_slice | solution.py:81
  127.9 6.0 %fusion.43 = f32[8,1,64,512]{3,2,0,1:T(8,128)S(1)} fusion(bf16[1,4096,512]{2,1,0:T(8,128)(2,1)} %param.25, bf16[8,1,64,4096]{3,2,1,0:T(8,128)(2,1)} %all-gather.9.cloned.1.call-done, f32[4096]{0:T(1024)S(1)} %copy-done.14, f32[8,64]{1,0:T(8,128)S(1)} %add_rsqrt_fusion.1), kind=kOutput, calls=%fused_computation.44 | convolution fusion | flops 2155872256 | bytes 9455616 | tf_op jit(solution)/shard_map/sxcd,xdf->sxcf/dot_general | solution.py:123
  138.8 61.9 %while.18 = (s32[]{:T(128)}, f32[384,4,2]{0,2,1:T(2,128)S(1)}, f32[384,4,2]{0,2,1:T(2,128)S(1)}, f32[384,4,2,128]{0,3,2,1:T(8,128)S(1)}, bf16[3072,512]{0,1:T(8,...) while((s32[]{:T(128)}, f32[384,4,2]{0,2,1:T(2,128)S(1)}, ...), condition=%wide.region_3.4_spmd.clone, body=%wide.region_0.3_spmd.clone.sunk | while | flops 1250443648 | bytes 99691728 | solution.py:92
  140.8 6.6 %fusion.86 = (f32[384,4,2]{0,2,1:T(2,128)S(1)}, f32[4,2,1024,384]{3,2,1,0:T(8,128)}) fusion(pred[384,1024]{0,1:T(8,128)(4,1)S(1)} %broadcast_compare_fusion.2, bf16[1024,4,2,64]{0,3,2,1:T(8,128)(2,1)S(1)} %bitcast.148, bf16[384,4,2,64]{0,3,2,1:T(8,128)(2,1)S(1)} %get-tuple-element.290), kind=kOutput, calls=%fused_computation.6.clone.1 | convolution fusion | flops 412087296 | bytes 14430208 | tf_op jit(solution)/shard_map/while/body/eval_jaxpr/ihcd,jhcd->ihcj/dot_general | solution.py:44
  147.5 6.9 %fusion.88 = f32[384,4,2]{0,2,1:T(2,128)S(1)} fusion(f32[4,2,1024,384]{3,2,1,0:T(8,128)} %get-tuple-element.257, f32[384,4,2]{0,2,1:T(2,128)S(1)} %fusion.87, pred[384,1024]{0,1:T(8,128)(4,1)S(1)} %broadcast_compare_fusion.2), kind=kLoop, calls=%fused_computation.8.clone.1 | loop fusion | flops 15725568 | bytes 13000704 | tf_op jit(solution)/shard_map/while/body/eval_jaxpr/reduce_sum | solution.py:55
  155.9 3.6 %bitcast_add_fusion.2 = f32[384,4,2,128]{0,3,2,1:T(8,128)S(1)} fusion(f32[384,4,2,128]{0,3,2,1:T(8,128)S(1)} %get-tuple-element.276, bf16[1024,4,128,1]{0,2,3,1:T(8,128)(2,1)S(1)} %bitcast.149, f32[4,2,1024,384]{3,2,1,0:T(8,128)S(1)} %copy-done, f32[384,4,2]{0,2,1:T(2,128)S(1)} %fusion.87, pred[384,1024]{0,1:T(8,128)(4,1)S(1)} %broadcast_compare_fusion.2, ...), kind=kOutput, calls=%fused_computation.11.clone.1 | convolution fusion | flops 822214656 | bytes 17195008 | tf_op jit(solution)/shard_map/while/body/eval_jaxpr/ihcj,jhe->ihce/dot_general | solution.py:56
  161.6 6.6 %fusion.86 = (f32[384,4,2]{0,2,1:T(2,128)S(1)}, f32[4,2,1024,384]{3,2,1,0:T(8,128)}) fusion(pred[384,1024]{0,1:T(8,128)(4,1)S(1)} %broadcast_compare_fusion.2, bf16[1024,4,2,64]{0,3,2,1:T(8,128)(2,1)S(1)} %bitcast.148, bf16[384,4,2,64]{0,3,2,1:T(8,128)(2,1)S(1)} %get-tuple-element.290), kind=kOutput, calls=%fused_computation.6.clone.1 | convolution fusion | flops 412087296 | bytes 14430208 | tf_op jit(solution)/shard_map/while/body/eval_jaxpr/ihcd,jhcd->ihcj/dot_general | solution.py:44
  168.2 6.8 %fusion.88 = f32[384,4,2]{0,2,1:T(2,128)S(1)} fusion(f32[4,2,1024,384]{3,2,1,0:T(8,128)} %get-tuple-element.257, f32[384,4,2]{0,2,1:T(2,128)S(1)} %fusion.87, pred[384,1024]{0,1:T(8,128)(4,1)S(1)} %broadcast_compare_fusion.2), kind=kLoop, calls=%fused_computation.8.clone.1 | loop fusion | flops 15725568 | bytes 13000704 | tf_op jit(solution)/shard_map/while/body/eval_jaxpr/reduce_sum | solution.py:55
  176.5 3.6 %bitcast_add_fusion.2 = f32[384,4,2,128]{0,3,2,1:T(8,128)S(1)} fusion(f32[384,4,2,128]{0,3,2,1:T(8,128)S(1)} %get-tuple-element.276, bf16[1024,4,128,1]{0,2,3,1:T(8,128)(2,1)S(1)} %bitcast.149, f32[4,2,1024,384]{3,2,1,0:T(8,128)S(1)} %copy-done, f32[384,4,2]{0,2,1:T(2,128)S(1)} %fusion.87, pred[384,1024]{0,1:T(8,128)(4,1)S(1)} %broadcast_compare_fusion.2, ...), kind=kOutput, calls=%fused_computation.11.clone.1 | convolution fusion | flops 822214656 | bytes 17195008 | tf_op jit(solution)/shard_map/while/body/eval_jaxpr/ihcj,jhe->ihce/dot_general | solution.py:56
  182.1 6.6 %fusion.86 = (f32[384,4,2]{0,2,1:T(2,128)S(1)}, f32[4,2,1024,384]{3,2,1,0:T(8,128)}) fusion(pred[384,1024]{0,1:T(8,128)(4,1)S(1)} %broadcast_compare_fusion.2, bf16[1024,4,2,64]{0,3,2,1:T(8,128)(2,1)S(1)} %bitcast.148, bf16[384,4,2,64]{0,3,2,1:T(8,128)(2,1)S(1)} %get-tuple-element.290), kind=kOutput, calls=%fused_computation.6.clone.1 | convolution fusion | flops 412087296 | bytes 14430208 | tf_op jit(solution)/shard_map/while/body/eval_jaxpr/ihcd,jhcd->ihcj/dot_general | solution.py:44
  188.8 6.8 %fusion.88 = f32[384,4,2]{0,2,1:T(2,128)S(1)} fusion(f32[4,2,1024,384]{3,2,1,0:T(8,128)} %get-tuple-element.257, f32[384,4,2]{0,2,1:T(2,128)S(1)} %fusion.87, pred[384,1024]{0,1:T(8,128)(4,1)S(1)} %broadcast_compare_fusion.2), kind=kLoop, calls=%fused_computation.8.clone.1 | loop fusion | flops 15725568 | bytes 13000704 | tf_op jit(solution)/shard_map/while/body/eval_jaxpr/reduce_sum | solution.py:55
  197.1 3.6 %bitcast_add_fusion.2 = f32[384,4,2,128]{0,3,2,1:T(8,128)S(1)} fusion(f32[384,4,2,128]{0,3,2,1:T(8,128)S(1)} %get-tuple-element.276, bf16[1024,4,128,1]{0,2,3,1:T(8,128)(2,1)S(1)} %bitcast.149, f32[4,2,1024,384]{3,2,1,0:T(8,128)S(1)} %copy-done, f32[384,4,2]{0,2,1:T(2,128)S(1)} %fusion.87, pred[384,1024]{0,1:T(8,128)(4,1)S(1)} %broadcast_compare_fusion.2, ...), kind=kOutput, calls=%fused_computation.11.clone.1 | convolution fusion | flops 822214656 | bytes 17195008 | tf_op jit(solution)/shard_map/while/body/eval_jaxpr/ihcj,jhe->ihce/dot_general | solution.py:56
  202.2 6.1 %fusion.38 = bf16[8,1,64,1024]{3,2,1,0:T(8,128)(2,1)} fusion(bf16[1,2048,1024]{2,1,0:T(8,128)(2,1)} %param.27, bf16[8,1,64,2048]{3,2,0,1:T(8,128)(2,1)} %all-gather.11.cloned.1.call-done), kind=kOutput, calls=%fused_computation.43 | convolution fusion | flops 2148007936 | bytes 7340032 | tf_op jit(solution)/shard_map/sxcf,xfd->sxcd/dot_general | solution.py:137
  208.4 3.6 %all-to-all-start.1 = ((bf16[8,1,64,1024]{3,2,1,0:T(8,128)(2,1)}), bf16[8,1,64,1024]{3,2,1,0:T(8,128)(2,1)S(1)}, u32[]{:S(2)}, u32[]{:S(2)}) async-start(bf16[8,1,64,1024]{3,2,1,0:T(8,128)(2,1)} %fusion.38), calls=%async_computation.1 | async-start | bytes 2097152 | tf_op jit(solution)/shard_map/all_to_all | solution.py:144
  212.1 20.6 %all-gather.7.cloned.1.call-done = bf16[1,1,384,2048]{2,3,1,0:T(8,128)(2,1)} async-done(((bf16[1,1,384,512]{2,3,1,0:T(8,128)(2,1)}), bf16[1,1,384,2048]{2,3,1,0:T(8,128)(2,1)}) %all-gather.7.cloned.1.call-update) | async-done | bytes 1572880 | tf_op jit(solution)/shard_map/all_gather | solution.py:130
  232.6 5.4 %fusion.35 = bf16[384,1024]{1,0:T(8,128)(2,1)} fusion(bf16[2048,1024]{1,0:T(8,128)(2,1)} %param.20, bf16[1,1,384,2048]{2,3,1,0:T(8,128)(2,1)} %all-gather.7.cloned.1.call-done), kind=kOutput, calls=%fused_computation.42 | convolution fusion | flops 1611005952 | bytes 6553600 | tf_op jit(solution)/shard_map/dot_general | solution.py:129
  (130 shorter events, 43.7 us)
Async XLA Ops:
  7.2 117.6 %all-gather.9.cloned.1.call-start = ((), (), s32[]{:S(2)}) async-start(), calls=%async_computation.4 | async-start | bytes 5242880 | tf_op jit(solution)/shard_map/all_gather | solution.py:122
  12.6 35.0 %copy-start.8 = (bf16[384,512]{1,0:T(8,128)(2,1)S(1)}, bf16[384,512]{1,0:T(8,128)(2,1)}, u32[]{:S(2)}) copy-start(bf16[384,512]{1,0:T(8,128)(2,1)} %param.17) | copy-start | bytes 1179652
  12.6 72.0 %copy-start.9 = (bf16[384,512]{1,0:T(8,128)(2,1)S(1)}, bf16[384,512]{1,0:T(8,128)(2,1)}, u32[]{:S(2)}) copy-start(bf16[384,512]{1,0:T(8,128)(2,1)} %param.16) | copy-start | bytes 1179652
  12.6 91.4 %copy-start.10 = (f32[4]{0:T(128)S(1)}, f32[4]{0:T(128)}, u32[]{:S(2)}) copy-start(f32[4]{0:T(128)} %param.18) | copy-start | bytes 52
  12.6 91.4 %copy-start.12 = (f32[128]{0:T(128)S(1)}, f32[128]{0:T(128)}, u32[]{:S(2)}) copy-start(f32[128]{0:T(128)} %param.19) | copy-start | bytes 1540
  47.5 91.2 %all-gather.5.cloned.1.call-start = ((), (), s32[]{:S(2)}) async-start(), calls=%async_computation.2 | async-start | bytes 3538944 | tf_op jit(solution)/shard_map/all_gather | solution.py:69
  47.8 9.1 %collective-permute-start = (bf16[384,512]{0,1:T(8,128)(2,1)S(1)}, bf16[384,512]{0,1:T(8,128)(2,1)S(1)}, u32[]{:S(2)}, u32[]{:S(2)}) collective-permute-start(bf16[384,512]{0,1:T(8,128)(2,1)S(1)} %copy.37), channel_id=1, source_target_pairs={{0,4},{4,8},{8,12},{12,16},{16,20},{20,24},{24,28},{28,0},{1,5},{5... | collective-permute-start | bytes 1179656 | tf_op jit(solution)/shard_map/ppermute | solution.py:77
  56.9 9.0 %collective-permute-start.1 = (bf16[384,512]{0,1:T(8,128)(2,1)S(1)}, bf16[384,512]{0,1:T(8,128)(2,1)S(1)}, u32[]{:S(2)}, u32[]{:S(2)}) collective-permute-start(bf16[384,512]{0,1:T(8,128)(2,1)S(1)} %collective-permute-done), channel_id=1, source_target_pairs={{0,4},{4,8},{8,12},{12,16},{16,20},{20,24},{24,28},{28,0},{1,5},{5... | collective-permute-start | bytes 1179656 | tf_op jit(solution)/shard_map/ppermute | solution.py:77
  65.9 9.0 %collective-permute-start.2 = (bf16[384,512]{0,1:T(8,128)(2,1)S(1)}, bf16[384,512]{0,1:T(8,128)(2,1)S(1)}, u32[]{:S(2)}, u32[]{:S(2)}) collective-permute-start(bf16[384,512]{0,1:T(8,128)(2,1)S(1)} %collective-permute-done.1), channel_id=1, source_target_pairs={{0,4},{4,8},{8,12},{12,16},{16,20},{20,24},{24,28},{28,0},{1,5},{5... | collective-permute-start | bytes 1179656 | tf_op jit(solution)/shard_map/ppermute | solution.py:77
  75.6 9.0 %collective-permute-start.3 = (bf16[384,512]{0,1:T(8,128)(2,1)S(1)}, bf16[384,512]{0,1:T(8,128)(2,1)S(1)}, u32[]{:S(2)}, u32[]{:S(2)}) collective-permute-start(bf16[384,512]{0,1:T(8,128)(2,1)S(1)} %collective-permute-done.2), channel_id=1, source_target_pairs={{0,4},{4,8},{8,12},{12,16},{16,20},{20,24},{24,28},{28,0},{1,5},{5... | collective-permute-start | bytes 1179656 | tf_op jit(solution)/shard_map/ppermute | solution.py:77
  84.6 18.1 %copy-start.4 = (bf16[384,512]{0,1:T(8,128)(2,1)}, bf16[384,512]{0,1:T(8,128)(2,1)S(1)}, u32[]{:S(2)}) copy-start(bf16[384,512]{0,1:T(8,128)(2,1)S(1)} %collective-permute-done.3) | copy-start | bytes 1179652
  84.6 9.0 %collective-permute-start.4 = (bf16[384,512]{0,1:T(8,128)(2,1)S(1)}, bf16[384,512]{0,1:T(8,128)(2,1)S(1)}, u32[]{:S(2)}, u32[]{:S(2)}) collective-permute-start(bf16[384,512]{0,1:T(8,128)(2,1)S(1)} %collective-permute-done.3), channel_id=1, source_target_pairs={{0,4},{4,8},{8,12},{12,16},{16,20},{20,24},{24,28},{28,0},{1,5},{5... | collective-permute-start | bytes 1179656 | tf_op jit(solution)/shard_map/ppermute | solution.py:77
  85.6 116.6 %all-gather.11.cloned.1.call-start = ((), (), s32[]{:S(2)}) async-start(), calls=%async_computation.5 | async-start | bytes 2621440 | tf_op jit(solution)/shard_map/all_gather | solution.py:139
  93.6 9.1 %copy-start.6 = (bf16[384,512]{0,1:T(8,128)(2,1)}, bf16[384,512]{0,1:T(8,128)(2,1)S(1)}, u32[]{:S(2)}) copy-start(bf16[384,512]{0,1:T(8,128)(2,1)S(1)} %collective-permute-done.4) | copy-start | bytes 1179652
  93.6 9.1 %collective-permute-start.5 = (bf16[384,512]{0,1:T(8,128)(2,1)S(1)}, bf16[384,512]{0,1:T(8,128)(2,1)}, u32[]{:S(2)}, u32[]{:S(2)}) collective-permute-start(bf16[384,512]{0,1:T(8,128)(2,1)S(1)} %collective-permute-done.4), channel_id=1, source_target_pairs={{0,4},{4,8},{8,12},{12,16},{16,20},{20,24},{24,28},{28,0},{1,5},{5... | collective-permute-start | bytes 1179656 | tf_op jit(solution)/shard_map/ppermute | solution.py:77
  102.7 9.4 %collective-permute-start.6 = (bf16[384,512]{0,1:T(8,128)(2,1)}, bf16[384,512]{0,1:T(8,128)(2,1)}, u32[]{:S(2)}, u32[]{:S(2)}) collective-permute-start(bf16[384,512]{0,1:T(8,128)(2,1)} %collective-permute-done.5), channel_id=1, source_target_pairs={{0,4},{4,8},{8,12},{12,16},{16,20},{20,24},{24,28},{28,0},{1,5},{5... | collective-permute-start | bytes 1179656 | tf_op jit(solution)/shard_map/ppermute | solution.py:77
  104.0 16.0 %copy-start.7 = (bf16[384,512]{0,1:T(8,128)(2,1)S(1)}, bf16[384,512]{0,1:T(8,128)(2,1)}, u32[]{:S(2)}) copy-start(bf16[384,512]{0,1:T(8,128)(2,1)} %copy-done.6) | copy-start | bytes 1179652
  104.0 16.1 %copy-start.5 = (bf16[384,512]{0,1:T(8,128)(2,1)S(1)}, bf16[384,512]{0,1:T(8,128)(2,1)}, u32[]{:S(2)}) copy-start(bf16[384,512]{0,1:T(8,128)(2,1)} %copy-done.4) | copy-start | bytes 1179652
  104.0 16.2 %copy-start.3 = (bf16[384,512]{0,1:T(8,128)(2,1)S(1)}, bf16[384,512]{0,1:T(8,128)(2,1)}, u32[]{:S(2)}) copy-start(bf16[384,512]{0,1:T(8,128)(2,1)} %copy-done.2) | copy-start | bytes 1179652
  137.3 95.4 %all-gather.7.cloned.1.call-start = ((), (), s32[]{:S(2)}) async-start(), calls=%async_computation.3 | async-start | bytes 1966080 | tf_op jit(solution)/shard_map/all_gather | solution.py:130
  147.5 8.5 %copy-start = (f32[4,2,1024,384]{3,2,1,0:T(8,128)S(1)}, f32[4,2,1024,384]{3,2,1,0:T(8,128)}, u32[]{:S(2)}) copy-start(f32[4,2,1024,384]{3,2,1,0:T(8,128)} %get-tuple-element.257) | copy-start | bytes 37748740 | tf_op jit(solution)/shard_map/while
  168.2 8.3 %copy-start = (f32[4,2,1024,384]{3,2,1,0:T(8,128)S(1)}, f32[4,2,1024,384]{3,2,1,0:T(8,128)}, u32[]{:S(2)}) copy-start(f32[4,2,1024,384]{3,2,1,0:T(8,128)} %get-tuple-element.257) | copy-start | bytes 37748740 | tf_op jit(solution)/shard_map/while
  202.2 9.7 %copy-start.11 = (f32[128,2]{0,1:T(2,128)S(1)}, f32[128,2]{0,1:T(2,128)}, u32[]{:S(2)}) copy-start(f32[128,2]{0,1:T(2,128)} %param.24) | copy-start | bytes 3076
  208.4 30.1 %all-to-all-start.1 = ((bf16[8,1,64,1024]{3,2,1,0:T(8,128)(2,1)}), bf16[8,1,64,1024]{3,2,1,0:T(8,128)(2,1)S(1)}, u32[]{:S(2)}, u32[]{:S(2)}) async-start(bf16[8,1,64,1024]{3,2,1,0:T(8,128)(2,1)} %fusion.38), calls=%async_computation.1 | async-start | bytes 2097152 | tf_op jit(solution)/shard_map/all_to_all | solution.py:144
  (5 other events, 28.7 us)
Sparse Core Ops, SparseCore 0:
  47.7 51.4 all-gather.8
  100.8 37.9 all-gather.4
  141.2 34.2 all-gather.10
  202.3 30.2 all-gather.6
